TPU v7x, 32 devices: a whole 2x2x4 slice. The times are simulated.
32 devices in a mesh: kv: 16 (over z, y, x), tp: 2 (over core).
Axes of the slice: x: 2, y: 2, z: 4, core: 2. Of those that a mesh axis runs over, the one named last changes fastest.
Arguments:
- tokens: bfloat16 [256, 2048], P('kv', 'tp'), may hold values from -20 to 20
- norm_gain: float32 [2048], replicated, may hold values from 0.1 to 1.9
- w_query: bfloat16 [2048, 1024], P(None, 'tp'), may hold values from -0.125 to 0.125
- w_key: bfloat16 [2048, 1024], P(None, 'tp'), may hold values from -0.125 to 0.125
- w_value: bfloat16 [2048, 1024], P(None, 'tp'), may hold values from -0.125 to 0.125
- w_outgate: bfloat16 [2048, 1024], P(None, 'tp'), may hold values from -0.125 to 0.125
- w_input_gate: bfloat16 [2048, 8], replicated, may hold values from -0.125 to 0.125
- w_forget_gate: bfloat16 [2048, 8], replicated, may hold values from -0.125 to 0.125
- memory: float32 [256, 8, 128, 128], P('kv', 'tp'), may hold values from -6 to 6
- normalizer: float32 [256, 8, 128], P('kv', 'tp'), may hold values from -6 to 6
- memory_max: float32 [256, 8], P('kv', 'tp'), may hold values from -2 to 300
- w_output: bfloat16 [1024, 2048], P(None, 'tp'), may hold values from -0.1875 to 0.1875
- ffn_gain: float32 [2048], P('tp'), may hold values from 0.1 to 1.9
- w_gate: bfloat16 [2048, 5632], P('tp', 'kv'), may hold values from -0.125 to 0.125
- w_up: bfloat16 [2048, 5632], P('tp', 'kv'), may hold values from -0.125 to 0.125
- w_down: bfloat16 [5632, 2048], P('kv', 'tp'), may hold values from -0.078125 to 0.078125
Outputs:
- result: bfloat16 [256, 2048], P('kv', 'tp')
- new_memory: float32 [256, 8, 128, 128], P('kv', 'tp')
- new_normalizer: float32 [256, 8, 128], P('kv', 'tp')
- new_max: float32 [256, 8], P('kv', 'tp')
All inputs are finite; a program needn't handle non-finite values.
Results may differ from a plain program's by a relative error of at most 0.013.
Values may be sent and summed in bfloat16 or wider, within the bound.
A program may use at most 64 MiB of HBM per device.

v0:
```python
import jax
import jax.numpy as jnp
from jax import lax
from jax.sharding import PartitionSpec as P

D = 2048


def activate(gate_sum, up_sum, square_sum):
    ffn_scale = lax.rsqrt(square_sum / D + 1e-06)[:, None]
    return (jax.nn.silu(ffn_scale * gate_sum) * (ffn_scale * up_sum)).astype(jnp.bfloat16)


def per_device(
    tokens,
    norm_gain,
    w_query,
    w_key,
    w_value,
    w_outgate,
    w_input_gate,
    w_forget_gate,
    memory,
    normalizer,
    memory_max,
    w_output,
    ffn_gain,
    w_gate,
    w_up,
    w_down,
):
    local_rows = tokens.shape[0]
    head_count = memory.shape[1]
    head_dim = memory.shape[2]
    full_rows = lax.all_gather(tokens, "tp", axis=1, tiled=True)
    rows_f = full_rows.astype(jnp.float32)
    row_scale = lax.rsqrt(jnp.mean(rows_f * rows_f, axis=-1, keepdims=True) + 1e-06)
    normed = (rows_f * row_scale * norm_gain).astype(jnp.bfloat16)

    def project(weight):
        return jnp.dot(normed, weight, preferred_element_type=jnp.float32).reshape(
            local_rows, head_count, head_dim
        )

    queries = project(w_query) * head_dim ** (-0.5)
    key_vec = project(w_key)
    values = project(w_value)
    outgate = project(w_outgate)
    first_head = lax.axis_index("tp") * head_count
    igate = lax.dynamic_slice_in_dim(
        jnp.dot(normed, w_input_gate, preferred_element_type=jnp.float32), first_head, head_count, 1
    )
    forget_pre = lax.dynamic_slice_in_dim(
        jnp.dot(normed, w_forget_gate, preferred_element_type=jnp.float32),
        first_head,
        head_count,
        1,
    )
    lforget = jax.nn.log_sigmoid(forget_pre)
    new_max = jnp.maximum(lforget + memory_max, igate)
    keep_weight = jnp.exp(lforget + memory_max - new_max)
    admit_weight = jnp.exp(igate - new_max)
    new_memory = keep_weight[..., None, None] * memory + admit_weight[..., None, None] * (
        key_vec[..., :, None] * values[..., None, :]
    )
    new_normalizer = keep_weight[..., None] * normalizer + admit_weight[..., None] * key_vec
    numerator = jnp.einsum("bhd,bhdv->bhv", queries, new_memory, precision=lax.Precision.HIGHEST)
    denominator = jnp.sum(queries * new_normalizer, axis=-1)
    cell_out = numerator / jnp.maximum(jnp.abs(denominator), jnp.exp(-new_max))[..., None]
    head_mean = jnp.mean(cell_out, axis=-1, keepdims=True)
    centered = cell_out - head_mean
    head_var = jnp.mean(centered * centered, axis=-1, keepdims=True)
    mixed = (
        (jax.nn.sigmoid(outgate) * centered * lax.rsqrt(head_var + 1e-05))
        .reshape(local_rows, head_count * head_dim)
        .astype(jnp.bfloat16)
    )
    branch_out = jnp.dot(
        lax.all_gather(mixed, "tp", axis=1, tiled=True),
        w_output,
        preferred_element_type=jnp.float32,
    )
    resid = (tokens.astype(jnp.float32) + branch_out).astype(jnp.bfloat16)
    every_row = lax.all_gather(resid, "kv", axis=0, tiled=True)
    every_f = every_row.astype(jnp.float32)
    square_part = jnp.sum(every_f * every_f, axis=-1)
    ffn_in = (every_f * ffn_gain).astype(jnp.bfloat16)
    gate_part = jnp.dot(ffn_in, w_gate, preferred_element_type=jnp.float32)
    up_part = jnp.dot(ffn_in, w_up, preferred_element_type=jnp.float32)
    gate_full, up_full, square_full = (
        lax.psum(gate_part.astype(jnp.bfloat16), "tp").astype(jnp.float32),
        lax.psum(up_part.astype(jnp.bfloat16), "tp").astype(jnp.float32),
        lax.psum(square_part.astype(jnp.bfloat16), "tp").astype(jnp.float32),
    )
    hidden = activate(gate_full, up_full, square_full)
    down_out = lax.psum_scatter(
        jnp.dot(hidden, w_down, preferred_element_type=jnp.float32),
        "kv",
        scatter_dimension=0,
        tiled=True,
    )
    result = (resid.astype(jnp.float32) + down_out).astype(jnp.bfloat16)
    return (result, new_memory, new_normalizer, new_max)


def solution(mesh):
    placed = (
        P("kv", "tp"),
        P(),
        P(None, "tp"),
        P(None, "tp"),
        P(None, "tp"),
        P(None, "tp"),
        P(),
        P(),
        P("kv", "tp", None, None),
        P("kv", "tp", None),
        P("kv", "tp"),
        P(None, "tp"),
        P("tp"),
        P("tp", "kv"),
        P("tp", "kv"),
        P("kv", "tp"),
    )
    return jax.shard_map(
        per_device,
        mesh=mesh,
        in_specs=placed,
        out_specs=(P("kv", "tp"), P("kv", "tp", None, None), P("kv", "tp", None), P("kv", "tp")),
        check_vma=False,
    )
```

profile of v0, /device:TPU:0, one launch (start us, length us, event | category | flops | bytes accessed | tf_op | source)
XLA Modules:
  0.0 181.3 jit_solution(10911743880774895137)
XLA Ops:
  7.2 0.0 copy-start
  7.2 0.0 copy-start.3
  7.2 0.0 copy-start.11
  7.2 0.0 copy-start.12
  7.2 0.0 copy-start.7
  7.2 0.0 all-reduce.3.cloned.1.call-start
  7.3 2.3 %all_gather.9 = bf16[16,2048]{1,0:T(8,128)(2,1)S(1)} all-gather(bf16[16,1024]{1,0:T(8,128)(2,1)} %param.16), channel_id=1, replica_groups=mesh['kv'=16,'tp'=2] {'tp'}, dimensions={1}, use_global_device_ids=true | all-gather | bytes 98304 | tf_op jit(solution)/shard_map/all_gather | solution.py:35
  9.6 0.1 fusion.11
  9.8 0.0 copy-start.5
  9.8 2.0 %convolution_multiply_fusion = f32[16,512]{1,0:T(8,128)S(1)} fusion(bf16[2048,512]{1,0:T(8,128)(2,1)} %param.18, bf16[16,2048]{1,0:T(8,128)(2,1)S(1)} %all_gather.9, f32[2048]{0:T(1024)} %param.17, f32[16]{0:T(128)S(1)} %add_rsqrt_fusion.2), kind=kOutput, calls=%fused_computation.7 | convolution fusion | flops 33693696 | bytes 2203712 | tf_op jit(solution)/shard_map/dot_general | solution.py:41
  11.9 0.0 copy-done.3
  11.9 0.0 copy-done.11
  11.9 0.2 fusion.21
  12.1 0.0 copy-done.12
  12.1 0.2 fusion.23
  12.3 0.0 copy-done.7
  12.3 0.0 copy-start.6
  12.3 0.1 copy.25
  12.4 0.1 copy.26
  12.5 2.0 %fusion.19 = f32[16,512]{1,0:T(8,128)S(1)} fusion(bf16[2048,512]{1,0:T(8,128)(2,1)} %param.19, bf16[16,2048]{1,0:T(8,128)(2,1)S(1)} %all_gather.9, f32[2048]{0:T(1024)S(1)} %copy-done.3, f32[16]{0:T(128)S(1)} %add_rsqrt_fusion.2), kind=kOutput, calls=%fused_computation.43 | convolution fusion | flops 33685504 | bytes 2203712 | tf_op jit(solution)/shard_map/dot_general | solution.py:41
  14.5 0.0 copy-done.5
  14.6 0.7 multiply_reduce_fusion.1
  15.3 0.1 copy.29
  15.4 0.1 copy.30
  15.4 0.0 copy-start.2
  15.5 2.2 %fusion.17 = f32[16,512]{1,0:T(8,128)S(1)} fusion(bf16[2048,512]{1,0:T(8,128)(2,1)} %param.20, bf16[16,2048]{1,0:T(8,128)(2,1)S(1)} %all_gather.9, f32[2048]{0:T(1024)S(1)} %copy-done.3, f32[16]{0:T(128)S(1)} %add_rsqrt_fusion.2), kind=kOutput, calls=%fused_computation.42 | convolution fusion | flops 33685504 | bytes 2203712 | tf_op jit(solution)/shard_map/dot_general | solution.py:41
  17.6 0.0 copy-done.6
  17.6 0.1 copy-done.2
  17.7 0.4 fusion.3
  18.2 3.7 %multiply_add_fusion = f32[16,4,128,128]{3,2,1,0:T(8,128)S(1)} fusion(f32[16,4,128,128]{3,2,1,0:T(8,128)} %param.24, f32[16,4,128]{2,1,0:T(4,128)S(1)} %mul.143, f32[16,4,128]{2,1,0:T(4,128)S(1)} %mul.141, f32[16,4]{1,0:T(8,128)S(1)} %copy.26, f32[16,4]{1,0:T(8,128)S(1)} %copy.25), kind=kLoop, calls=%fused_computation | loop fusion | flops 4194304 | bytes 8454656 | tf_op jit(solution)/shard_map/add | solution.py:63
  21.9 0.0 copy-start.1
  21.9 0.0 copy-start.4
  21.9 3.7 %fusion.28 = f32[16,4,1,128]{3,2,1,0:T(1,128)S(1)} fusion(f32[16,4,128,1]{2,3,1,0:T(1,128)S(1)} %bitcast.20, f32[16,4,128,128]{3,2,1,0:T(8,128)S(1)} %multiply_add_fusion), kind=kOutput, calls=%fused_computation.47 | convolution fusion | flops 12582912 | bytes 4259840 | tf_op jit(solution)/shard_map/bhd,bhdv->bhv/dot_general | solution.py:67
  25.6 0.0 copy-done.1
  25.6 0.0 copy-start.8
  25.6 0.0 copy-start.13
  25.6 0.2 fusion.27
  25.8 0.2 multiply_reduce_fusion
  26.0 0.1 multiply_convert_fusion.2
  26.1 1.8 %all_gather.10 = bf16[16,1024]{1,0:T(8,128)(2,1)S(1)} all-gather(bf16[16,512]{1,0:T(8,128)(2,1)S(1)} %bitcast.22), channel_id=1, replica_groups=mesh['kv'=16,'tp'=2] {'tp'}, dimensions={1}, use_global_device_ids=true | all-gather | bytes 49152 | tf_op jit(solution)/shard_map/all_gather | solution.py:79
  27.9 0.0 copy-done
  27.9 0.0 copy-done.4
  27.9 0.0 copy-start.9
  27.9 0.4 fusion
  28.3 45.4 %all_gather.11 = bf16[256,1024]{1,0:T(8,128)(2,1)S(1)} all-gather(bf16[16,1024]{1,0:T(8,128)(2,1)S(1)} %fusion), channel_id=1, replica_groups=mesh['kv'=16,'tp'=2] {'kv'}, dimensions={0}, use_global_device_ids=true | all-gather | bytes 557056 | tf_op jit(solution)/shard_map/all_gather | solution.py:84
  73.7 0.0 copy-done.8
  73.7 0.0 copy-done.13
  73.7 0.0 copy-start.10
  73.7 1.1 convolution_convert_fusion
  74.8 0.0 copy-done.9
  74.8 1.1 convolution_convert_fusion.1
  75.8 0.0 all-reduce.3.cloned.1.call-update
  75.9 0.0 reduce-scatter.2.cloned.1.call-start
  75.9 0.2 fusion.4
  76.1 2.5 %psum.21 = bf16[256]{0:T(256)(128)(2,1)S(1)} all-reduce(bf16[256]{0:T(256)(128)(2,1)S(1)} %fusion.4), channel_id=1, replica_groups=mesh['kv'=16,'tp'=2] {'tp'}, use_global_device_ids=true, to_apply=%region_5.6 | all-reduce | flops 256 | bytes 1024 | tf_op jit(solution)/shard_map/psum | solution.py:93
  78.6 11.7 %all-reduce.3.cloned.1.call-done = (bf16[256,352]{0,1:T(8,128)(2,1)}, bf16[256,352]{0,1:T(8,128)(2,1)}) async-done(((bf16[256,352]{0,1:T(8,128)(2,1)}, bf16[256,352]{0,1:T(8,128)(2,1)}), (bf16[256,352]{0,1:T(8,128)(2,1)}, bf16[256,352]{0,1:T(8,128)(2,1)})) %all-reduce.3.cloned.1.call-update) | async-done | bytes 360464 | tf_op jit(solution)/shard_map/psum | solution.py:92
  90.3 0.0 copy-done.10
  90.3 2.5 %fusion.8 = f32[256,1024]{1,0:T(8,128)} fusion(bf16[352,1024]{1,0:T(8,128)(2,1)S(1)} %copy-done.10, bf16[256,352]{0,1:T(8,128)(2,1)} %get-tuple-element.4, bf16[256,352]{0,1:T(8,128)(2,1)} %get-tuple-element.5, f32[256]{0:T(256)S(1)} %add_rsqrt_fusion.1), kind=kOutput, calls=%fused_computation.15 | convolution fusion | flops 185450496 | bytes 2130944 | tf_op jit(solution)/shard_map/dot_general | solution.py:97
  92.9 0.0 reduce-scatter.2.cloned.1.call-update
  92.9 80.1 %reduce-scatter.2.cloned.1.call-done = f32[16,1024]{1,0:T(8,128)} async-done(((f32[256,1024]{1,0:T(8,128)}), f32[16,1024]{1,0:T(8,128)}) %reduce-scatter.2.cloned.1.call-update) | async-done | bytes 65552 | tf_op jit(solution)/shard_map/reduce_scatter | solution.py:96
  173.0 1.5 add_convert_fusion
  (13 shorter events, 0.2 us)
Async XLA Ops:
  7.2 20.7 %copy-start = (bf16[1024,1024]{1,0:T(8,128)(2,1)S(1)}, bf16[1024,1024]{1,0:T(8,128)(2,1)}, u32[]{:S(2)}) copy-start(bf16[1024,1024]{1,0:T(8,128)(2,1)} %param.27) | copy-start | bytes 6291460
  7.2 4.7 %copy-start.3 = (f32[2048]{0:T(1024)S(1)}, f32[2048]{0:T(1024)}, u32[]{:S(2)}) copy-start(f32[2048]{0:T(1024)} %param.17) | copy-start | bytes 24580
  7.2 4.7 %copy-start.11 = (bf16[2048,8]{0,1:T(8,128)(2,1)S(1)}, bf16[2048,8]{0,1:T(8,128)(2,1)}, u32[]{:S(2)}) copy-start(bf16[2048,8]{0,1:T(8,128)(2,1)} %param.22) | copy-start | bytes 98308
  7.2 4.9 %copy-start.12 = (bf16[2048,8]{0,1:T(8,128)(2,1)S(1)}, bf16[2048,8]{0,1:T(8,128)(2,1)}, u32[]{:S(2)}) copy-start(bf16[2048,8]{0,1:T(8,128)(2,1)} %param.23) | copy-start | bytes 98308
  7.2 5.1 %copy-start.7 = (f32[16,4]{0,1:T(4,128)S(1)}, f32[16,4]{0,1:T(4,128)}, u32[]{:S(2)}) copy-start(f32[16,4]{0,1:T(4,128)} %param.26) | copy-start | bytes 772
  7.2 83.1 %all-reduce.3.cloned.1.call-start = ((), (), s32[]{:S(2)}) async-start(), calls=%async_computation.2 | async-start | bytes 720896 | tf_op jit(solution)/shard_map/psum | solution.py:92
  9.8 4.8 %copy-start.5 = (f32[16,4,128]{2,1,0:T(4,128)S(1)}, f32[16,4,128]{2,1,0:T(4,128)}, u32[]{:S(2)}) copy-start(f32[16,4,128]{2,1,0:T(4,128)} %param.25) | copy-start | bytes 98308
  12.3 5.3 %copy-start.6 = (f32[16,4]{0,1:T(4,128)}, f32[16,4]{0,1:T(4,128)S(1)}, u32[]{:S(2)}) copy-start(f32[16,4]{0,1:T(4,128)S(1)} %get-tuple-element.11) | copy-start | bytes 772
  15.4 2.2 %copy-start.2 = (bf16[2048,512]{1,0:T(8,128)(2,1)S(1)}, bf16[2048,512]{1,0:T(8,128)(2,1)}, u32[]{:S(2)}) copy-start(bf16[2048,512]{1,0:T(8,128)(2,1)} %param.21) | copy-start | bytes 6291460
  21.9 3.7 %copy-start.1 = (f32[16,4,128,128]{3,2,1,0:T(8,128)}, f32[16,4,128,128]{3,2,1,0:T(8,128)S(1)}, u32[]{:S(2)}) copy-start(f32[16,4,128,128]{3,2,1,0:T(8,128)S(1)} %multiply_add_fusion) | copy-start | bytes 12582916
  21.9 6.0 %copy-start.4 = (bf16[16,1024]{1,0:T(8,128)(2,1)S(1)}, bf16[16,1024]{1,0:T(8,128)(2,1)}, u32[]{:S(2)}) copy-start(bf16[16,1024]{1,0:T(8,128)(2,1)} %param.16) | copy-start | bytes 98308
  25.6 48.1 %copy-start.8 = (bf16[1024,352]{0,1:T(8,128)(2,1)S(1)}, bf16[1024,352]{0,1:T(8,128)(2,1)}, u32[]{:S(2)}) copy-start(bf16[1024,352]{0,1:T(8,128)(2,1)} %param.30) | copy-start | bytes 2162692
  25.6 48.1 %copy-start.13 = (f32[1024]{0:T(1024)S(1)}, f32[1024]{0:T(1024)}, u32[]{:S(2)}) copy-start(f32[1024]{0:T(1024)} %param.28) | copy-start | bytes 12292
  27.9 46.9 %copy-start.9 = (bf16[1024,352]{0,1:T(8,128)(2,1)S(1)}, bf16[1024,352]{0,1:T(8,128)(2,1)}, u32[]{:S(2)}) copy-start(bf16[1024,352]{0,1:T(8,128)(2,1)} %param.29) | copy-start | bytes 2162692
  73.7 16.6 %copy-start.10 = (bf16[352,1024]{1,0:T(8,128)(2,1)S(1)}, bf16[352,1024]{1,0:T(8,128)(2,1)}, u32[]{:S(2)}) copy-start(bf16[352,1024]{1,0:T(8,128)(2,1)} %param.31) | copy-start | bytes 2162692
  75.9 97.1 %reduce-scatter.2.cloned.1.call-start = ((), (), s32[]{:S(2)}) async-start(), calls=%async_computation.1 | async-start | bytes 1114112 | tf_op jit(solution)/shard_map/reduce_scatter | solution.py:96
Sparse Core Ops, SparseCore 0:
  76.0 14.2 all-reduce.2
  93.0 79.9 reduce-scatter.1
where the time goes:
time: 182 us; the launch traced here: 181 us
  waiting for transfers between devices  91.8 us (50%)
  blocking collectives  52 us (29%)
  matrix products  15.8 us (9%)
  between operations  14.3 us (8%)
  other arithmetic  6.72 us (4%)
    reduce_scatter x1, waiting for transfers between devices, per_device(): lax.psum_scatter(jnp.dot(hidden, w_down, preferred_element_type=jnp.float...  80.1 us
    all_gather x1, blocking collectives, per_device(): every_row = lax.all_gather(resid, 'kv', axis=0, tiled=True)  45.4 us
    psum x1, waiting for transfers between devices, per_device(): lax.psum(up_part.astype(jnp.bfloat16), 'tp').astype(jnp.float32)  11.7 us
    dot_general x4, matrix products, project(): jnp.dot(normed, weight, preferred_element_type=jnp.float32)  6.65 us
    add x1, other arithmetic, per_device(): keep_weight[..., None, None] * memory  3.72 us
    dot_general x1, matrix products, per_device(): jnp.einsum('bhd,bhdv->bhv', queries, new_memory, precision=lax.Precision....  3.66 us
  transfers between devices with their start and end apart: 2, of which 2 were waited for; matrix products, arithmetic and copies ran while one was open for 0% of the time, Pallas kernels for 0%

commit v1 on v0

--- a/solution.py
+++ b/solution.py
@@ -81,7 +81,9 @@
         preferred_element_type=jnp.float32,
     )
     resid = (tokens.astype(jnp.float32) + branch_out).astype(jnp.bfloat16)
-    every_row = lax.all_gather(resid, "kv", axis=0, tiled=True)
+    every_row = jnp.concatenate(
+        lax.all_to_all(jnp.stack([resid] * lax.axis_size("kv")), "kv", 0, 0), axis=0
+    )
     every_f = every_row.astype(jnp.float32)
     square_part = jnp.sum(every_f * every_f, axis=-1)
     ffn_in = (every_f * ffn_gain).astype(jnp.bfloat16)

time: 182 us -> 163 us (0.90)
  blocking collectives: 52 us -> 30.2 us
  waiting for transfers between devices: 91.8 us -> 94.3 us
    all_gather x1 -> x0, blocking collectives: 45.4 us -> none  [per_device(): every_row = lax.all_gather(resid, 'kv', axis=0, tiled=True)]
    all_to_all x0 -> x1, blocking collectives: none -> 23.5 us  [per_device(): lax.all_to_all(jnp.stack([resid] * lax.axis_size('kv')), 'kv', 0, 0)]
    psum x1, waiting for transfers between devices: 11.7 us -> 14.1 us  [per_device(): lax.psum(up_part.astype(jnp.bfloat16), 'tp').astype(jnp.float32)]
where the time goes in v1:
time: 163 us; the launch traced here: 162 us
  waiting for transfers between devices  94.3 us (58%)
  blocking collectives  30.2 us (19%)
  matrix products  15.8 us (10%)
  between operations  14.3 us (9%)
  other arithmetic  6.83 us (4%)
    reduce_scatter x1, waiting for transfers between devices, per_device(): lax.psum_scatter(jnp.dot(hidden, w_down, preferred_element_type=jnp.float...  80.1 us
    all_to_all x1, blocking collectives, per_device(): lax.all_to_all(jnp.stack([resid] * lax.axis_size('kv')), 'kv', 0, 0)  23.5 us
    psum x1, waiting for transfers between devices, per_device(): lax.psum(up_part.astype(jnp.bfloat16), 'tp').astype(jnp.float32)  14.1 us
    dot_general x4, matrix products, project(): jnp.dot(normed, weight, preferred_element_type=jnp.float32)  6.65 us
    add x1, other arithmetic, per_device(): keep_weight[..., None, None] * memory  3.72 us
    dot_general x1, matrix products, per_device(): jnp.einsum('bhd,bhdv->bhv', queries, new_memory, precision=lax.Precision....  3.66 us
  transfers between devices with their start and end apart: 2, of which 2 were waited for; matrix products, arithmetic and copies ran while one was open for 0% of the time, Pallas kernels for 0%

profile of v1, /device:TPU:0, one launch (start us, length us, event | category | flops | bytes accessed | tf_op | source)
XLA Modules:
  0.0 162.1 jit_solution(9474226026971016227)
XLA Ops:
  7.2 0.0 copy-start
  7.2 0.0 copy-start.5
  7.2 0.0 copy-start.12
  7.2 0.0 copy-start.13
  7.2 0.0 copy-start.10
  7.2 0.0 all-reduce.3.cloned.1.call-start
  7.3 2.3 %all_gather.6 = bf16[16,2048]{1,0:T(8,128)(2,1)S(1)} all-gather(bf16[16,1024]{1,0:T(8,128)(2,1)} %param.16), channel_id=1, replica_groups=mesh['kv'=16,'tp'=2] {'tp'}, dimensions={1}, use_global_device_ids=true | all-gather | bytes 98304 | tf_op jit(solution)/shard_map/all_gather | solution.py:35
  9.6 0.1 fusion.8
  9.8 0.0 copy-start.7
  9.8 2.0 %convolution_multiply_fusion = f32[16,512]{1,0:T(8,128)S(1)} fusion(bf16[2048,512]{1,0:T(8,128)(2,1)} %param.18, bf16[16,2048]{1,0:T(8,128)(2,1)S(1)} %all_gather.6, f32[2048]{0:T(1024)} %param.17, f32[16]{0:T(128)S(1)} %add_rsqrt_fusion.2), kind=kOutput, calls=%fused_computation.5 | convolution fusion | flops 33693696 | bytes 2203712 | tf_op jit(solution)/shard_map/dot_general | solution.py:41
  11.9 0.0 copy-done.5
  11.9 0.0 copy-done.12
  11.9 0.2 fusion.18
  12.1 0.0 copy-done.13
  12.1 0.2 fusion.20
  12.3 0.0 copy-done.10
  12.3 0.0 copy-start.8
  12.3 0.1 copy.31
  12.4 0.1 copy.32
  12.5 2.0 %fusion.16 = f32[16,512]{1,0:T(8,128)S(1)} fusion(bf16[2048,512]{1,0:T(8,128)(2,1)} %param.19, bf16[16,2048]{1,0:T(8,128)(2,1)S(1)} %all_gather.6, f32[2048]{0:T(1024)S(1)} %copy-done.5, f32[16]{0:T(128)S(1)} %add_rsqrt_fusion.2), kind=kOutput, calls=%fused_computation.42 | convolution fusion | flops 33685504 | bytes 2203712 | tf_op jit(solution)/shard_map/dot_general | solution.py:41
  14.5 0.0 copy-done.7
  14.6 0.7 multiply_reduce_fusion.2
  15.3 0.1 copy.35
  15.4 0.1 copy.36
  15.4 0.0 copy-start.2
  15.5 2.2 %fusion.14 = f32[16,512]{1,0:T(8,128)S(1)} fusion(bf16[2048,512]{1,0:T(8,128)(2,1)} %param.20, bf16[16,2048]{1,0:T(8,128)(2,1)S(1)} %all_gather.6, f32[2048]{0:T(1024)S(1)} %copy-done.5, f32[16]{0:T(128)S(1)} %add_rsqrt_fusion.2), kind=kOutput, calls=%fused_computation.41 | convolution fusion | flops 33685504 | bytes 2203712 | tf_op jit(solution)/shard_map/dot_general | solution.py:41
  17.6 0.0 copy-done.8
  17.6 0.1 copy-done.2
  17.7 0.4 fusion.3
  18.2 3.7 %multiply_add_fusion = f32[16,4,128,128]{3,2,1,0:T(8,128)S(1)} fusion(f32[16,4,128,128]{3,2,1,0:T(8,128)} %param.24, f32[16,4,128]{2,1,0:T(4,128)S(1)} %mul.144, f32[16,4,128]{2,1,0:T(4,128)S(1)} %mul.142, f32[16,4]{1,0:T(8,128)S(1)} %copy.32, f32[16,4]{1,0:T(8,128)S(1)} %copy.31), kind=kLoop, calls=%fused_computation | loop fusion | flops 4194304 | bytes 8454656 | tf_op jit(solution)/shard_map/add | solution.py:63
  21.9 0.0 copy-start.1
  21.9 0.0 copy-start.6
  21.9 3.7 %fusion.25 = f32[16,4,1,128]{3,2,1,0:T(1,128)S(1)} fusion(f32[16,4,128,1]{2,3,1,0:T(1,128)S(1)} %bitcast.26, f32[16,4,128,128]{3,2,1,0:T(8,128)S(1)} %multiply_add_fusion), kind=kOutput, calls=%fused_computation.46 | convolution fusion | flops 12582912 | bytes 4259840 | tf_op jit(solution)/shard_map/bhd,bhdv->bhv/dot_general | solution.py:67
  25.6 0.0 copy-done.1
  25.6 0.0 copy-start.9
  25.6 0.2 fusion.24
  25.8 0.2 multiply_reduce_fusion.1
  26.0 0.1 multiply_convert_fusion.2
  26.1 1.8 %all_gather.7 = bf16[16,1024]{1,0:T(8,128)(2,1)S(1)} all-gather(bf16[16,512]{1,0:T(8,128)(2,1)S(1)} %bitcast.28), channel_id=1, replica_groups=mesh['kv'=16,'tp'=2] {'tp'}, dimensions={1}, use_global_device_ids=true | all-gather | bytes 49152 | tf_op jit(solution)/shard_map/all_gather | solution.py:79
  27.9 0.0 copy-done
  27.9 0.0 copy-done.6
  27.9 0.0 copy-start.3
  27.9 0.4 fusion
  28.3 0.0 copy-start.4
  28.3 0.1 stack.2
  28.4 23.5 %all_to_all.5 = bf16[16,16,1024]{2,1,0:T(8,128)(2,1)S(1)} all-to-all(bf16[16,16,1024]{2,1,0:T(8,128)(2,1)S(1)} %stack.2), channel_id=1, replica_groups=mesh['kv'=16,'tp'=2] {'kv'}, dimensions={0} | all-to-all | bytes 1048576 | tf_op jit(solution)/shard_map/all_to_all | solution.py:85
  51.9 0.0 copy-done.9
  51.9 0.1 fusion.4
  52.0 0.0 copy-done.3
  52.0 0.0 copy-start.11
  52.1 1.1 convolution_convert_fusion
  53.1 0.0 copy-done.4
  53.1 1.1 convolution_convert_fusion.1
  54.2 0.0 all-reduce.3.cloned.1.call-update
  54.2 0.0 reduce-scatter.2.cloned.1.call-start
  54.3 0.2 multiply_reduce_fusion
  54.4 0.1 convert_element_type.69
  54.5 2.5 %psum.21 = bf16[256]{0:T(256)(128)(2,1)S(1)} all-reduce(bf16[256]{0:T(256)(128)(2,1)S(1)} %convert_element_type.69), channel_id=1, replica_groups=mesh['kv'=16,'tp'=2] {'tp'}, use_global_device_ids=true, to_apply=%region_5.6 | all-reduce | flops 256 | bytes 1024 | tf_op jit(solution)/shard_map/psum | solution.py:95
  57.0 14.1 %all-reduce.3.cloned.1.call-done = (bf16[256,352]{0,1:T(8,128)(2,1)}, bf16[256,352]{0,1:T(8,128)(2,1)}) async-done(((bf16[256,352]{0,1:T(8,128)(2,1)}, bf16[256,352]{0,1:T(8,128)(2,1)}), (bf16[256,352]{0,1:T(8,128)(2,1)}, bf16[256,352]{0,1:T(8,128)(2,1)})) %all-reduce.3.cloned.1.call-update) | async-done | bytes 360464 | tf_op jit(solution)/shard_map/psum | solution.py:94
  71.1 0.0 copy-done.11
  71.1 2.5 %fusion.5 = f32[256,1024]{1,0:T(8,128)} fusion(bf16[352,1024]{1,0:T(8,128)(2,1)S(1)} %copy-done.11, bf16[256,352]{0,1:T(8,128)(2,1)} %get-tuple-element.4, bf16[256,352]{0,1:T(8,128)(2,1)} %get-tuple-element.5, f32[256]{0:T(256)S(1)} %add_rsqrt_fusion.1), kind=kOutput, calls=%fused_computation.14 | convolution fusion | flops 185450496 | bytes 2130944 | tf_op jit(solution)/shard_map/dot_general | solution.py:99
  73.7 0.0 reduce-scatter.2.cloned.1.call-update
  73.7 80.1 %reduce-scatter.2.cloned.1.call-done = f32[16,1024]{1,0:T(8,128)} async-done(((f32[256,1024]{1,0:T(8,128)}), f32[16,1024]{1,0:T(8,128)}) %reduce-scatter.2.cloned.1.call-update) | async-done | bytes 65552 | tf_op jit(solution)/shard_map/reduce_scatter | solution.py:98
  153.8 1.5 add_convert_fusion
  (13 shorter events, 0.2 us)
Async XLA Ops:
  7.2 20.7 %copy-start = (bf16[1024,1024]{1,0:T(8,128)(2,1)S(1)}, bf16[1024,1024]{1,0:T(8,128)(2,1)}, u32[]{:S(2)}) copy-start(bf16[1024,1024]{1,0:T(8,128)(2,1)} %param.27) | copy-start | bytes 6291460
  7.2 4.7 %copy-start.5 = (f32[2048]{0:T(1024)S(1)}, f32[2048]{0:T(1024)}, u32[]{:S(2)}) copy-start(f32[2048]{0:T(1024)} %param.17) | copy-start | bytes 24580
  7.2 4.7 %copy-start.12 = (bf16[2048,8]{0,1:T(8,128)(2,1)S(1)}, bf16[2048,8]{0,1:T(8,128)(2,1)}, u32[]{:S(2)}) copy-start(bf16[2048,8]{0,1:T(8,128)(2,1)} %param.22) | copy-start | bytes 98308
  7.2 4.9 %copy-start.13 = (bf16[2048,8]{0,1:T(8,128)(2,1)S(1)}, bf16[2048,8]{0,1:T(8,128)(2,1)}, u32[]{:S(2)}) copy-start(bf16[2048,8]{0,1:T(8,128)(2,1)} %param.23) | copy-start | bytes 98308
  7.2 5.1 %copy-start.10 = (f32[16,4]{0,1:T(4,128)S(1)}, f32[16,4]{0,1:T(4,128)}, u32[]{:S(2)}) copy-start(f32[16,4]{0,1:T(4,128)} %param.26) | copy-start | bytes 772
  7.2 63.9 %all-reduce.3.cloned.1.call-start = ((), (), s32[]{:S(2)}) async-start(), calls=%async_computation.3 | async-start | bytes 720896 | tf_op jit(solution)/shard_map/psum | solution.py:94
  9.8 4.8 %copy-start.7 = (f32[16,4,128]{2,1,0:T(4,128)S(1)}, f32[16,4,128]{2,1,0:T(4,128)}, u32[]{:S(2)}) copy-start(f32[16,4,128]{2,1,0:T(4,128)} %param.25) | copy-start | bytes 98308
  12.3 5.3 %copy-start.8 = (f32[16,4]{0,1:T(4,128)}, f32[16,4]{0,1:T(4,128)S(1)}, u32[]{:S(2)}) copy-start(f32[16,4]{0,1:T(4,128)S(1)} %get-tuple-element.11) | copy-start | bytes 772
  15.4 2.2 %copy-start.2 = (bf16[2048,512]{1,0:T(8,128)(2,1)S(1)}, bf16[2048,512]{1,0:T(8,128)(2,1)}, u32[]{:S(2)}) copy-start(bf16[2048,512]{1,0:T(8,128)(2,1)} %param.21) | copy-start | bytes 6291460
  21.9 3.7 %copy-start.1 = (f32[16,4,128,128]{3,2,1,0:T(8,128)}, f32[16,4,128,128]{3,2,1,0:T(8,128)S(1)}, u32[]{:S(2)}) copy-start(f32[16,4,128,128]{3,2,1,0:T(8,128)S(1)} %multiply_add_fusion) | copy-start | bytes 12582916
  21.9 6.0 %copy-start.6 = (bf16[16,1024]{1,0:T(8,128)(2,1)S(1)}, bf16[16,1024]{1,0:T(8,128)(2,1)}, u32[]{:S(2)}) copy-start(bf16[16,1024]{1,0:T(8,128)(2,1)} %param.16) | copy-start | bytes 98308
  25.6 26.3 %copy-start.9 = (f32[1024]{0:T(1024)S(1)}, f32[1024]{0:T(1024)}, u32[]{:S(2)}) copy-start(f32[1024]{0:T(1024)} %param.28) | copy-start | bytes 12292
  27.9 24.1 %copy-start.3 = (bf16[1024,352]{0,1:T(8,128)(2,1)S(1)}, bf16[1024,352]{0,1:T(8,128)(2,1)}, u32[]{:S(2)}) copy-start(bf16[1024,352]{0,1:T(8,128)(2,1)} %param.30) | copy-start | bytes 2162692
  28.3 24.8 %copy-start.4 = (bf16[1024,352]{0,1:T(8,128)(2,1)S(1)}, bf16[1024,352]{0,1:T(8,128)(2,1)}, u32[]{:S(2)}) copy-start(bf16[1024,352]{0,1:T(8,128)(2,1)} %param.29) | copy-start | bytes 2162692
  52.0 19.1 %copy-start.11 = (bf16[352,1024]{1,0:T(8,128)(2,1)S(1)}, bf16[352,1024]{1,0:T(8,128)(2,1)}, u32[]{:S(2)}) copy-start(bf16[352,1024]{1,0:T(8,128)(2,1)} %param.31) | copy-start | bytes 2162692
  54.2 99.6 %reduce-scatter.2.cloned.1.call-start = ((), (), s32[]{:S(2)}) async-start(), calls=%async_computation.2 | async-start | bytes 1114112 | tf_op jit(solution)/shard_map/reduce_scatter | solution.py:98
Sparse Core Ops, SparseCore 0:
  54.3 16.7 all-reduce.2
  73.8 79.9 reduce-scatter.1
